TPU v7x, 32 devices: a whole 2x2x4 slice. The times are simulated.
32 devices in a mesh: sp: 8 (over z, x), tp: 4 (over y, core).
Axes of the slice: x: 2, y: 2, z: 4, core: 2. Of those that a mesh axis runs over, the one named last changes fastest.
Arguments:
- query: bfloat16 [2048, 1024], P('sp', 'tp'), may hold values from -6 to 6
- forget_logits: bfloat16 [2048, 1024], P('sp', 'tp'), may hold values from -5.5 to 5.5
- written_values: bfloat16 [2048, 1024], P('sp', 'tp'), may hold values from -6 to 6
- output_gate_logits: bfloat16 [2048, 1024], P('sp', 'tp'), may hold values from -6 to 6
- forget_floor_gap: float32 [1024], P('tp'), may hold values from 0 to 0.08
- extra_log_decay: float32 [2048, 1024], P('sp', 'tp'), may hold values from -0.7 to 0
- head_norm_gain: float32 [128], replicated, may hold values from 0.1 to 1.9
- output_weight: bfloat16 [1024, 2048], P('tp'), may hold values from -0.1875 to 0.1875
- residual: bfloat16 [2048, 2048], P(('sp', 'tp')), may hold values from -6 to 6
- mixer_norm_gain: float32 [2048], replicated, may hold values from 0.1 to 1.9
- mixer_up_weight: bfloat16 [2048, 8192], P('sp', 'tp'), may hold values from -0.125 to 0.125
- mixer_down_weight: bfloat16 [8192, 2048], P(('tp', 'sp')), may hold values from -0.0625 to 0.0625
Outputs:
- layer_out: bfloat16 [2048, 2048], P(('sp', 'tp'))
All inputs are finite; a program needn't handle non-finite values.
Results may differ from a plain program's by a relative error of at most 0.015.
Values may be sent and summed in bfloat16 or wider, within the bound.
A program may use at most 128 MiB of HBM per device.

v0:
```python
import jax
import jax.numpy as jnp
from jax import lax
from jax.sharding import PartitionSpec as P

HEAD_K = 128
HEAD_V = 128
BLOCK = 64


norm_eps = 1e-06
highest_precision = lax.Precision.HIGHEST


def carried_in(part, axis, combine, identity):
    place = lax.axis_index(axis)
    gathered = jax.tree.map(lambda a: lax.all_gather(a, axis), part)
    state = jax.tree.map(lambda a, e: jnp.zeros_like(a) + jnp.asarray(e, a.dtype), part, identity)

    def one(step, state):
        return combine(
            state, jax.tree.map(lambda a: lax.dynamic_index_in_dim(a, step, 0, False), gathered)
        )

    return lax.fori_loop(0, place, one, state)


def block_update(carry_forward_state, block_inputs):
    query_rows_block, gate_rows_block, value_rows_block, log_block = block_inputs
    cumulative_log = jnp.cumsum(log_block, axis=1)
    length = query_rows_block.shape[1]
    causal = jnp.arange(length)[:, None] >= jnp.arange(length)[None, :]
    across_blocks = jnp.einsum(
        "dcj,djw->dcw",
        query_rows_block * jnp.exp(cumulative_log),
        carry_forward_state,
        precision=highest_precision,
    )
    spread = cumulative_log[:, :, None, :] - cumulative_log[:, None, :, :]
    decay_table = jnp.exp(jnp.where(causal[None, :, :, None], spread, -jnp.inf))
    scores = jnp.einsum(
        "htk,hsk,htsk->hts",
        query_rows_block,
        gate_rows_block,
        decay_table,
        precision=highest_precision,
    )
    within = jnp.einsum("hts,hsv->htv", scores, value_rows_block, precision=highest_precision)
    final_log_total = cumulative_log[:, -1:, :]
    updated_state = jnp.exp(final_log_total[:, 0, :])[
        :, :, None
    ] * carry_forward_state + jnp.einsum(
        "tri,trw->tiw",
        gate_rows_block * jnp.exp(final_log_total - cumulative_log),
        value_rows_block,
        precision=highest_precision,
    )
    return (updated_state, across_blocks + within)


def to_blocks(array, inner):
    length = array.shape[0]
    split_up = array.reshape(length // BLOCK, BLOCK, array.shape[1] // inner, inner)
    return jnp.transpose(split_up, (0, 2, 1, 3))


def from_blocks(blocked):
    joined = jnp.transpose(blocked, (0, 2, 1, 3))
    return joined.reshape(joined.shape[0] * joined.shape[1], joined.shape[2], joined.shape[3])


def prepare_inputs(query, forget_logits, written_values, forget_floor_gap, extra_log_decay):
    input_gate_value = forget_floor_gap[None, :] * jax.nn.sigmoid(
        -forget_logits.astype(jnp.float32)
    )
    forget_log_rate = jnp.log1p(-input_gate_value) + extra_log_decay
    scaled_values = query.astype(jnp.float32) * HEAD_K ** (-0.5)
    return (scaled_values, input_gate_value, written_values.astype(jnp.float32), forget_log_rate)


def gate_out(recurrent, output_gate_logits, head_norm_gain):
    normal_part = recurrent * lax.rsqrt(
        jnp.mean(recurrent * recurrent, axis=-1, keepdims=True) + norm_eps
    )
    gating = jax.nn.silu(output_gate_logits.astype(jnp.float32)).reshape(recurrent.shape)
    mixed = normal_part * head_norm_gain * gating
    return mixed.reshape(recurrent.shape[0], -1).astype(jnp.bfloat16)


def normalize(stream, gain):
    scaled_rows = stream * lax.rsqrt(jnp.mean(stream * stream, axis=-1, keepdims=True) + norm_eps)
    return (scaled_rows * gain).astype(jnp.bfloat16)


def chain_states(earlier, later):
    return (earlier[0] + later[0], jnp.exp(later[0])[:, :, None] * earlier[1] + later[1])


def on_device(
    query,
    forget_logits,
    written_values,
    output_gate_logits,
    forget_floor_gap,
    extra_log_decay,
    head_norm_gain,
    output_weight,
    residual,
    mixer_norm_gain,
    mixer_up_weight,
    mixer_down_weight,
):
    scaled_values, input_gate_value, value_rows, forget_log_rate = prepare_inputs(
        query, forget_logits, written_values, forget_floor_gap, extra_log_decay
    )
    row_count, local_width = query.shape
    head_count = local_width // HEAD_K
    start_state = jnp.zeros((head_count, HEAD_K, HEAD_V), jnp.float32)
    local_state, blocked = lax.scan(
        block_update,
        start_state,
        (
            to_blocks(scaled_values, HEAD_K),
            to_blocks(input_gate_value, HEAD_K),
            to_blocks(value_rows, HEAD_V),
            to_blocks(forget_log_rate, HEAD_K),
        ),
    )
    log_total = jnp.sum(forget_log_rate, axis=0).reshape(head_count, HEAD_K)
    arrived_state = carried_in(
        (log_total, local_state),
        "sp",
        chain_states,
        (jnp.zeros_like(log_total), jnp.zeros_like(local_state)),
    )
    running = jnp.cumsum(forget_log_rate, axis=0)
    reached_state = (scaled_values * jnp.exp(running)).reshape(row_count, head_count, HEAD_K)
    carried_over = jnp.einsum(
        "cja,jae->cje", reached_state, arrived_state[1], precision=highest_precision
    )
    mixed = gate_out(from_blocks(blocked) + carried_over, output_gate_logits, head_norm_gain)
    stream_own = lax.psum_scatter(
        jnp.dot(mixed, output_weight, preferred_element_type=jnp.float32).astype(jnp.bfloat16),
        "tp",
        scatter_dimension=0,
        tiled=True,
    ).astype(jnp.float32) + residual.astype(jnp.float32)
    normed = lax.all_gather(normalize(stream_own, mixer_norm_gain), "tp", axis=0, tiled=True)
    columns = normed
    lifted = jnp.dot(
        columns,
        lax.all_gather(mixer_up_weight, "sp", axis=0, tiled=True),
        preferred_element_type=jnp.float32,
    )
    hidden = jnp.square(jax.nn.relu(lifted)).astype(jnp.bfloat16)
    columns = hidden
    projected = jnp.dot(
        columns,
        lax.all_gather(mixer_down_weight, "sp", axis=0, tiled=True),
        preferred_element_type=jnp.float32,
    )
    mlp_own = lax.psum_scatter(
        projected.astype(jnp.bfloat16), "tp", scatter_dimension=0, tiled=True
    ).astype(jnp.float32)
    return (stream_own + mlp_own).astype(jnp.bfloat16)


def solution(mesh):
    return jax.shard_map(
        on_device,
        mesh=mesh,
        in_specs=(
            P("sp", "tp"),
            P("sp", "tp"),
            P("sp", "tp"),
            P("sp", "tp"),
            P("tp"),
            P("sp", "tp"),
            P(),
            P("tp", None),
            P(("sp", "tp"), None),
            P(),
            P("sp", "tp"),
            P(("tp", "sp"), None),
        ),
        out_specs=P(("sp", "tp"), None),
        check_vma=False,
    )
```

profile of v0, /device:TPU:0, one launch (start us, length us, event | category | flops | bytes accessed | tf_op | source)
XLA Modules:
  0.0 423.6 jit_solution(12700383612470924152)
XLA Ops:
  6.5 1.3 fusion.25
  7.9 0.1 reshape.80
  8.0 0.2 fusion.22
  8.4 1.0 bitcast_multiply_fusion.5
  9.3 0.1 reshape.83
  9.5 0.1 reshape.81
  9.6 0.1 reshape.89
  9.8 22.5 %while.26 = (s32[]{:T(128)}, f32[2,128,128]{2,1,0:T(8,128)S(1)}, f32[4,2,64,128]{3,2,0,1:T(8,128)S(1)}, f32[4,2,64,128]{3,1,2,0:T(2,128)S(1)}, f32[4,2,64,128]{3...) while((s32[]{:T(128)}, f32[2,128,128]{2,1,0:T(8,128)S(1)}, ...), condition=%wide.region_2.3_spmd.clone, body=%wide.region_0.2_spmd.clone.sunk | while | flops 69382144 | bytes 10729600 | solution.py:119
  9.8 0.1 reduce_window_sum.28
  9.9 0.8 select_exponential_fusion.2
  10.8 3.6 fusion.42
  14.4 0.2 fusion.41
  14.6 0.3 fusion.43
  15.0 0.4 convolution_add_fusion.3
  15.6 0.8 select_exponential_fusion.2
  16.5 3.6 fusion.42
  20.0 0.2 fusion.41
  20.3 0.3 fusion.43
  20.6 0.4 convolution_add_fusion.3
  21.2 0.8 select_exponential_fusion.2
  22.1 3.6 fusion.42
  25.6 0.2 fusion.41
  25.9 0.3 fusion.43
  26.2 0.4 convolution_add_fusion.3
  26.8 0.8 select_exponential_fusion.2
  27.7 3.6 fusion.42
  31.3 0.2 fusion.41
  31.5 0.3 fusion.43
  31.9 0.4 convolution_add_fusion.3
  32.3 0.6 copy-done.1
  33.0 0.1 copy.55
  33.3 0.1 copy.56
  33.4 22.3 %all_gather.18 = f32[8,2,128]{2,1,0:T(2,128)S(1)} all-gather(f32[1,2,128]{2,1,0:T(2,128)S(1)} %bitcast.124), channel_id=1, replica_groups=mesh['sp'=8,'tp'=4] {'sp'}, dimensions={0}, use_global_device_ids=true | all-gather | bytes 9216 | tf_op jit(solution)/shard_map/all_gather | solution.py:17
  55.7 20.4 %all-gather.12.cloned.1.call-done = f32[16,128,128]{2,1,0:T(8,128)} async-done(((f32[2,128,128]{2,1,0:T(8,128)}), f32[16,128,128]{2,1,0:T(8,128)}) %all-gather.12.cloned.1.call-update) | async-done | bytes 1048592 | tf_op jit(solution)/shard_map/all_gather | solution.py:17
  76.1 0.4 multiply_reduce_fusion.1
  76.7 1.4 convolution_convert_fusion
  78.2 31.1 %reduce-scatter.3.cloned.1.call-done = bf16[64,2048]{1,0:T(8,128)(2,1)} async-done(((bf16[256,2048]{1,0:T(8,128)(2,1)}), bf16[64,2048]{1,0:T(8,128)(2,1)}) %reduce-scatter.3.cloned.1.call-update) | async-done | bytes 262160 | tf_op jit(solution)/shard_map/reduce_scatter | solution.py:142
  109.4 1.1 multiply_reduce_fusion
  110.5 1.8 multiply_convert_fusion
  112.4 0.5 all-gather.10.cloned.1.call-update
  113.0 0.5 all-gather.8.cloned.1.call-update
  113.5 0.2 reduce-scatter.5.cloned.1.call-start
  113.7 15.5 %all-gather.6.cloned.1.call-done = bf16[256,2048]{1,0:T(8,128)(2,1)} async-done(((bf16[64,2048]{1,0:T(8,128)(2,1)}), bf16[256,2048]{1,0:T(8,128)(2,1)}) %all-gather.6.cloned.1.call-update) | async-done | bytes 1048592 | tf_op jit(solution)/shard_map/all_gather | solution.py:148
  129.2 126.5 %all-gather.10.cloned.1.call-done = bf16[2048,2048]{1,0:T(8,128)(2,1)} async-done(((bf16[256,2048]{1,0:T(8,128)(2,1)}), bf16[2048,2048]{1,0:T(8,128)(2,1)}) %all-gather.10.cloned.1.call-update) | async-done | bytes 8388624 | tf_op jit(solution)/shard_map/all_gather | solution.py:159
  255.7 124.7 %all-gather.8.cloned.1.call-done = bf16[2048,2048]{1,0:T(8,128)(2,1)} async-done(((bf16[256,2048]{1,0:T(8,128)(2,1)}), bf16[2048,2048]{1,0:T(8,128)(2,1)}) %all-gather.8.cloned.1.call-update) | async-done | bytes 8388624 | tf_op jit(solution)/shard_map/all_gather | solution.py:152
  380.4 11.5 %convolution_convert_fusion.1 = bf16[256,2048]{1,0:T(8,128)(2,1)} fusion(bf16[2048,2048]{1,0:T(8,128)(2,1)} %all-gather.10.cloned.1.call-done, bf16[256,2048]{1,0:T(8,128)(2,1)} %all-gather.6.cloned.1.call-done, bf16[2048,2048]{1,0:T(8,128)(2,1)} %all-gather.8.cloned.1.call-done), kind=kOutput, calls=%fused_computation.35 | convolution fusion | flops 4297064448 | bytes 18874368 | tf_op jit(solution)/shard_map/dot_general | solution.py:157
  391.9 23.1 %reduce-scatter.5.cloned.1.call-done = bf16[64,2048]{1,0:T(8,128)(2,1)} async-done(((bf16[256,2048]{1,0:T(8,128)(2,1)}), bf16[64,2048]{1,0:T(8,128)(2,1)}) %reduce-scatter.5.cloned.1.call-update) | async-done | bytes 262160 | tf_op jit(solution)/shard_map/reduce_scatter | solution.py:162
  415.0 1.7 add_convert_fusion
  (73 shorter events, 1.2 us)
Async XLA Ops:
  6.5 70.2 %copy-start = (bf16[256,2048]{1,0:T(8,128)(2,1)S(1)}, bf16[256,2048]{1,0:T(8,128)(2,1)}, u32[]{:S(2)}) copy-start(bf16[256,2048]{1,0:T(8,128)(2,1)} %param.23) | copy-start | bytes 3145732
  6.5 3.1 copy-start.4
  6.5 69.6 %all-gather.12.cloned.1.call-start = ((), (), s32[]{:S(2)}) async-start(), calls=%async_computation.7 | async-start | bytes 1179648 | tf_op jit(solution)/shard_map/all_gather | solution.py:17
  9.8 23.4 %copy-start.5 = (bf16[256,256]{1,0:T(8,128)(2,1)S(1)}, bf16[256,256]{1,0:T(8,128)(2,1)}, u32[]{:S(2)}) copy-start(bf16[256,256]{1,0:T(8,128)(2,1)} %param.19) | copy-start | bytes 393220
  32.3 0.7 copy-start.1
  32.3 44.3 %copy-start.7 = (f32[128]{0:T(128)S(1)}, f32[128]{0:T(128)}, u32[]{:S(2)}) copy-start(f32[128]{0:T(128)} %param.22) | copy-start | bytes 1540
  33.0 76.4 %reduce-scatter.3.cloned.1.call-start = ((), (), s32[]{:S(2)}) async-start(), calls=%async_computation.2 | async-start | bytes 1310720 | tf_op jit(solution)/shard_map/reduce_scatter | solution.py:142
  33.0 76.4 %copy-start.2 = (bf16[64,2048]{1,0:T(8,128)(2,1)S(1)}, bf16[64,2048]{1,0:T(8,128)(2,1)}, u32[]{:S(2)}) copy-start(bf16[64,2048]{1,0:T(8,128)(2,1)} %param.24) | copy-start | bytes 786436
  33.3 77.3 %copy-start.6 = (f32[2048]{0:T(1024)S(1)}, f32[2048]{0:T(1024)}, u32[]{:S(2)}) copy-start(f32[2048]{0:T(1024)} %param.25) | copy-start | bytes 24580
  78.2 51.0 %all-gather.6.cloned.1.call-start = ((), (), s32[]{:S(2)}) async-start(), calls=%async_computation.3 | async-start | bytes 1310720 | tf_op jit(solution)/shard_map/all_gather | solution.py:148
  112.3 143.4 %all-gather.10.cloned.1.call-start = ((), (), s32[]{:S(2)}) async-start(), calls=%async_computation.5 | async-start | bytes 9437184 | tf_op jit(solution)/shard_map/all_gather | solution.py:159
  112.9 267.4 %all-gather.8.cloned.1.call-start = ((), (), s32[]{:S(2)}) async-start(), calls=%async_computation.4 | async-start | bytes 9437184 | tf_op jit(solution)/shard_map/all_gather | solution.py:152
  113.5 301.6 %copy-start.3 = (bf16[64,2048]{1,0:T(8,128)(2,1)S(1)}, bf16[64,2048]{1,0:T(8,128)(2,1)}, u32[]{:S(2)}) copy-start(bf16[64,2048]{1,0:T(8,128)(2,1)} %reduce-scatter.3.cloned.1.call-done) | copy-start | bytes 786436
  113.5 301.5 %reduce-scatter.5.cloned.1.call-start = ((), (), s32[]{:S(2)}) async-start(), calls=%async_computation.6 | async-start | bytes 1310720 | tf_op jit(solution)/shard_map/reduce_scatter | solution.py:162
Sparse Core Ops, SparseCore 0:
  33.1 42.9 all-gather.11
  78.6 30.6 reduce-scatter.2
  112.4 16.7 all-gather.5
  131.2 124.4 all-gather.9
  257.7 122.6 all-gather.7
  392.0 22.9 reduce-scatter.4
where the time goes:
time: 424 us
  waiting for transfers between devices  342 us (81%)
  other arithmetic  25.4 us (6%)
  blocking collectives  22.3 us (5%)
  matrix products  17.2 us (4%)
  between operations  13.7 us (3%)
    all_gather x1, waiting for transfers between devices, on_device(): lax.all_gather(mixer_down_weight, 'sp', axis=0, tiled=True)  126 us
    all_gather x1, waiting for transfers between devices, on_device(): lax.all_gather(mixer_up_weight, 'sp', axis=0, tiled=True)  125 us
    reduce_scatter x1, waiting for transfers between devices, on_device(): lax.psum_scatter(jnp.dot(mixed, output_weight, preferred_element_type=jnp...  31.1 us
    reduce_scatter x1, waiting for transfers between devices, on_device(): lax.psum_scatter(projected.astype(jnp.bfloat16), 'tp', scatter_dimension=...  23.1 us
    all_gather x1, blocking collectives, carried_in(): gathered = jax.tree.map(lambda a: lax.all_gather(a, axis), part)  22.3 us
    all_gather x1, waiting for transfers between devices, carried_in(): gathered = jax.tree.map(lambda a: lax.all_gather(a, axis), part)  20.4 us
    all_gather x1, waiting for transfers between devices, on_device(): lax.all_gather(normalize(stream_own, mixer_norm_gain), 'tp', axis=0, tile...  15.5 us
    dot_general x4, other arithmetic, block_update(): jnp.einsum('htk,hsk,htsk->hts', query_rows_block, gate_rows_block, decay_...  14.2 us
  transfers between devices with their start and end apart: 6, of which 6 were waited for; matrix products, arithmetic and copies ran while one was open for 0% of the time, Pallas kernels for 0%

commit v1 on v0

--- a/solution.py
+++ b/solution.py
@@ -1,6 +1,10 @@
+import functools
+
 import jax
 import jax.numpy as jnp
 from jax import lax
+from jax.experimental import pallas as pl
+from jax.experimental.pallas import tpu as pltpu
 from jax.sharding import PartitionSpec as P
 
 HEAD_K = 128
@@ -96,7 +100,245 @@
     return (earlier[0] + later[0], jnp.exp(later[0])[:, :, None] * earlier[1] + later[1])
 
 
+OUTER = 4
+LO = 2
+MESH = pl.DeviceIdType.MESH
+
+
+def mixer_kernel(
+    sp_size, tp_size,
+    mixed_ref, wo_ref, res_ref, gain_ref, up_ref, down_ref, out_ref,
+    pbuf, stream, s5, r5, s6, r6, nb, acc, s1, r1, s2, r2, acc2, s3, r3,
+    sem5s, sem5r, sem6s, sem6r, zs, zr, hs, hr, ls, lr, ls2, lr2,
+    q1s, q1r, q2s, q2r, q3s, q3r,
+):
+    outer, inner, hi = OUTER, sp_size // OUTER, tp_size // LO
+    sp, tp = lax.axis_index("sp"), lax.axis_index("tp")
+    o, i = lax.div(sp, inner), lax.rem(sp, inner)
+    h, l = lax.div(tp, LO), lax.rem(tp, LO)
+    other = 1 - l
+    rows, depth = res_ref.shape
+
+    def dev(oo, hh, ll):
+        return (oo * inner + i, hh * LO + ll)
+
+    def at_o(k):
+        return lax.rem(o + k, outer)
+
+    def from_o(k):
+        return lax.rem(o - k + outer, outer)
+
+    def at_h(m):
+        return lax.rem(h + m, hi)
+
+    def from_h(m):
+        return lax.rem(h - m + hi, hi)
+
+    def rcopy(src, dst, ssem, rsem, device):
+        return pltpu.make_async_remote_copy(
+            src_ref=src, dst_ref=dst, send_sem=ssem, recv_sem=rsem,
+            device_id=device, device_id_type=MESH,
+        )
+
+    barrier = pltpu.get_barrier_semaphore()
+    peers = [dev(at_o(k), h, l) for k in range(1, outer)]
+    peers += [dev(o, at_h(m), l) for m in range(1, hi)] + [dev(o, h, other)]
+    for peer in peers:
+        pl.semaphore_signal(barrier, inc=1, device_id=peer, device_id_type=MESH)
+    pl.semaphore_wait(barrier, len(peers))
+
+    branch = jnp.dot(mixed_ref[...], wo_ref[...], preferred_element_type=jnp.float32)
+    pbuf[...] = branch.reshape(tp_size, rows, depth)
+    for hh in range(hi):
+        s5[hh] = pbuf[hh * LO + other].astype(jnp.bfloat16)
+    c5 = rcopy(s5, r5, sem5s, sem5r, dev(o, h, other))
+    c5.start()
+    c5.wait_recv()
+    c6 = []
+    for m in range(1, hi):
+        to = at_h(m)
+        s6[m] = (pbuf[to * LO + l] + r5[to].astype(jnp.float32)).astype(jnp.bfloat16)
+        c = rcopy(s6.at[m], r6.at[m], sem6s.at[m], sem6r.at[m], dev(o, to, l))
+        c.start()
+        c6.append(c)
+    total = pbuf[tp] + r5[h].astype(jnp.float32) + res_ref[...].astype(jnp.float32)
+    for m in range(1, hi):
+        c6[m - 1].wait_recv()
+        total = total + r6[m].astype(jnp.float32)
+    stream[...] = total
+    scale = lax.rsqrt(jnp.mean(total * total, axis=-1, keepdims=True) + norm_eps)
+    nb[o, tp] = (total * scale * gain_ref[...]).astype(jnp.bfloat16)
+
+    def z_copy(k):
+        return rcopy(nb.at[o, tp], nb.at[o, tp], zs.at[k], zr.at[k], dev(at_o(k), h, l))
+
+    def h_copy(k, m):
+        ref = nb.at[from_o(k), tp]
+        return rcopy(ref, ref, hs.at[k, m], hr.at[k, m], dev(o, at_h(m), l))
+
+    def l_copy(k):
+        ref = nb.at[from_o(k), tp]
+        return rcopy(ref, ref, ls.at[k], lr.at[k], dev(o, h, other))
+
+    def l2_copy(k, m):
+        ref = nb.at[from_o(k), from_h(m) * LO + l]
+        return rcopy(ref, ref, ls2.at[k, m], lr2.at[k, m], dev(o, h, other))
+
+    def s1_copy(k):
+        return rcopy(s1.at[k], r1.at[k], q1s.at[k], q1r.at[k], dev(o, h, other))
+
+    def s2_copy(k, m):
+        return rcopy(s2.at[k, m], r2.at[k, m], q2s.at[k, m], q2r.at[k, m], dev(o, at_h(m), l))
+
+    def s3_copy(k):
+        return rcopy(s3.at[k], r3.at[k], q3s.at[k], q3r.at[k], dev(from_o(k), h, l))
+
+    for k in range(1, outer):
+        z_copy(k).start()
+
+    def forward(k):
+        for m in range(1, hi):
+            h_copy(k, m).start()
+        l_copy(k).start()
+
+    forward(0)
+
+    def body(j, carry):
+        @pl.when(j + 1 < outer)
+        def _():
+            z_copy(j + 1).wait_recv()
+            forward(j + 1)
+
+        @pl.when(j < outer)
+        def _():
+            for m in range(1, hi):
+                h_copy(j, m).wait_recv()
+                l2_copy(j, m).start()
+            l_copy(j).wait_recv()
+            for m in range(1, hi):
+                l2_copy(j, m).wait_recv()
+            x = nb[from_o(j)].reshape(tp_size * rows, depth)
+            lifted = jnp.dot(x, up_ref[...], preferred_element_type=jnp.float32)
+            hidden = jnp.square(jnp.maximum(lifted, 0.0)).astype(jnp.bfloat16)
+            part = jnp.dot(hidden, down_ref[...], preferred_element_type=jnp.float32)
+            pbuf[...] = part.reshape(tp_size, rows, depth)
+            for hh in range(hi):
+                s1[j, hh] = pbuf[hh * LO + other].astype(jnp.bfloat16)
+            s1_copy(j).start()
+            for hh in range(hi):
+                acc[j, hh] = pbuf[hh * LO + l]
+
+        @pl.when((j >= 1) & (j < outer + 1))
+        def _():
+            k = j - 1
+            s1_copy(k).wait_recv()
+            for m in range(1, hi):
+                to = at_h(m)
+                s2[k, m] = (acc[k, to] + r1[k, to].astype(jnp.float32)).astype(jnp.bfloat16)
+                s2_copy(k, m).start()
+            acc2[k] = acc[k, h] + r1[k, h].astype(jnp.float32)
+
+        @pl.when(j >= 2)
+        def _():
+            k = j - 2
+            v = acc2[k]
+            for m in range(1, hi):
+                s2_copy(k, m).wait_recv()
+                v = v + r2[k, m].astype(jnp.float32)
+            @pl.when(k == 0)
+            def _():
+                acc2[0] = v
+
+            @pl.when(k > 0)
+            def _():
+                s3[k] = v.astype(jnp.bfloat16)
+                s3_copy(k).start()
+
+        return carry
+
+    lax.fori_loop(0, outer + 2, body, 0)
+    final = stream[...] + acc2[0]
+    for k in range(1, outer):
+        s3_copy(k).wait_recv()
+        final = final + r3[k].astype(jnp.float32)
+    out_ref[...] = final.astype(jnp.bfloat16)
+
+    c5.wait_send()
+    for c in c6:
+        c.wait_send()
+    for k in range(outer):
+        if k > 0:
+            z_copy(k).wait_send()
+            s3_copy(k).wait_send()
+        l_copy(k).wait_send()
+        s1_copy(k).wait_send()
+        for m in range(1, hi):
+            h_copy(k, m).wait_send()
+            l2_copy(k, m).wait_send()
+            s2_copy(k, m).wait_send()
+
+
+def mixer(sp_size, tp_size, mixed, wo, res, gain, up, down):
+    rows, depth = res.shape
+    hi = tp_size // LO
+    f32, b16 = jnp.float32, jnp.bfloat16
+    dma = pltpu.SemaphoreType.DMA
+    vm = pltpu.VMEM
+    O = OUTER
+    return pl.pallas_call(
+        functools.partial(mixer_kernel, sp_size, tp_size),
+        out_shape=jax.ShapeDtypeStruct((rows, depth), b16),
+        in_specs=[pl.BlockSpec(memory_space=pltpu.VMEM)] * 6,
+        out_specs=pl.BlockSpec(memory_space=pltpu.VMEM),
+        scratch_shapes=[
+            vm((tp_size, rows, depth), f32),
+            vm((rows, depth), f32),
+            vm((hi, rows, depth), b16), vm((hi, rows, depth), b16),
+            vm((hi, rows, depth), b16), vm((hi, rows, depth), b16),
+            vm((O, tp_size, rows, depth), b16),
+            vm((O, hi, rows, depth), f32),
+            vm((O, hi, rows, depth), b16), vm((O, hi, rows, depth), b16),
+            vm((O, hi, rows, depth), b16), vm((O, hi, rows, depth), b16),
+            vm((O, rows, depth), f32),
+            vm((O, rows, depth), b16), vm((O, rows, depth), b16),
+            dma, dma, dma((hi,)), dma((hi,)),
+            dma((O,)), dma((O,)), dma((O, hi)), dma((O, hi)),
+            dma((O,)), dma((O,)), dma((O, hi)), dma((O, hi)),
+            dma((O,)), dma((O,)), dma((O, hi)), dma((O, hi)),
+            dma((O,)), dma((O,)),
+        ],
+        compiler_params=pltpu.CompilerParams(
+            collective_id=0, has_side_effects=True, vmem_limit_bytes=60 * 1024 * 1024
+        ),
+    )(mixed, wo, res, gain.reshape(1, depth), up, down)
+
+
+def regroup_weights(sp_size, up, down):
+    inner = sp_size // OUTER
+    inner_groups = [[o * inner + i for i in range(inner)] for o in range(OUTER)]
+    down_own = lax.all_gather(down, "sp", axis=0, tiled=True, axis_index_groups=inner_groups)
+    depth_part, cols = up.shape
+    width = cols // OUTER
+    o = lax.div(lax.axis_index("sp"), inner)
+    pieces = []
+    for k in range(OUTER):
+        to = lax.rem(o + k, OUTER)
+        piece = lax.dynamic_slice_in_dim(up, to * width, width, 1)
+        if k:
+            perm = [(s, (s + k * inner) % sp_size) for s in range(sp_size)]
+            piece = lax.ppermute(piece, "sp", perm)
+        pieces.append(piece)
+    stacked = jnp.stack(pieces)
+    both = lax.all_gather(stacked, "sp", axis=0, tiled=False, axis_index_groups=inner_groups)
+    order = lax.rem(o - jnp.arange(OUTER) + OUTER, OUTER)
+    both = jnp.take(both, order, axis=1)
+    full = jnp.transpose(both, (1, 0, 2, 3)).reshape(sp_size * depth_part, width)
+    return full, down_own
+
+
 def on_device(
+    sp_size,
+    tp_size,
     query,
     forget_logits,
     written_values,
@@ -139,35 +381,15 @@
         "cja,jae->cje", reached_state, arrived_state[1], precision=highest_precision
     )
     mixed = gate_out(from_blocks(blocked) + carried_over, output_gate_logits, head_norm_gain)
-    stream_own = lax.psum_scatter(
-        jnp.dot(mixed, output_weight, preferred_element_type=jnp.float32).astype(jnp.bfloat16),
-        "tp",
-        scatter_dimension=0,
-        tiled=True,
-    ).astype(jnp.float32) + residual.astype(jnp.float32)
-    normed = lax.all_gather(normalize(stream_own, mixer_norm_gain), "tp", axis=0, tiled=True)
-    columns = normed
-    lifted = jnp.dot(
-        columns,
-        lax.all_gather(mixer_up_weight, "sp", axis=0, tiled=True),
-        preferred_element_type=jnp.float32,
-    )
-    hidden = jnp.square(jax.nn.relu(lifted)).astype(jnp.bfloat16)
-    columns = hidden
-    projected = jnp.dot(
-        columns,
-        lax.all_gather(mixer_down_weight, "sp", axis=0, tiled=True),
-        preferred_element_type=jnp.float32,
-    )
-    mlp_own = lax.psum_scatter(
-        projected.astype(jnp.bfloat16), "tp", scatter_dimension=0, tiled=True
-    ).astype(jnp.float32)
-    return (stream_own + mlp_own).astype(jnp.bfloat16)
+    up_own, down_own = regroup_weights(sp_size, mixer_up_weight, mixer_down_weight)
+    return mixer(
+        sp_size, tp_size, mixed, output_weight, residual, mixer_norm_gain, up_own, down_own
+    )
 
 
 def solution(mesh):
     return jax.shard_map(
-        on_device,
+        functools.partial(on_device, mesh.shape["sp"], mesh.shape["tp"]),
         mesh=mesh,
         in_specs=(
             P("sp", "tp"),

time: 424 us -> 247 us (0.58)
  waiting for transfers between devices: 342 us -> 88.8 us
  Pallas kernels: 0 us -> 84.9 us
  matrix products: 17.2 us -> 4.22 us
  starting transfers between devices: 0.38 us -> 6.23 us
  local copies, waits for them, and re-layouts: 1.77 us -> 7.46 us
    all_gather x3 -> x2, waiting for transfers between devices: 267 us -> 62.6 us  [the longest x1 31.8 us: regroup_weights(): lax.all_gather(stacked, 'sp', axis=0, tiled=False, axis_index_groups=inne...]
    pallas_call x0 -> x1, Pallas kernels: none -> 84.9 us  [mixer(): pl.pallas_call(functools.partial(mixer_kernel, sp_size, tp_size), out_sha...]
    reduce_scatter x2 -> x0, waiting for transfers between devices: 54.3 us -> none  [the longest x1 31.1 us: on_device(): lax.psum_scatter(jnp.dot(mixed, output_weight, preferred_element_type=jnp...]
    ppermute x0 -> x3, waiting for transfers between devices: none -> 25.5 us  [regroup_weights(): piece = lax.ppermute(piece, 'sp', perm)]
    all_gather x1, waiting for transfers between devices: 20.4 us -> 0.01 us  [carried_in(): gathered = jax.tree.map(lambda a: lax.all_gather(a, axis), part)]
    dot_general x2 -> x0, matrix products: 13 us -> none  [the longest x1 11.5 us: on_device(): jnp.dot(columns, lax.all_gather(mixer_down_weight, 'sp', axis=0, tiled=Tr...]
    ppermute x0 -> x3, starting transfers between devices: none -> 6.14 us  [regroup_weights(): piece = lax.ppermute(piece, 'sp', perm)]
  transfers between devices with their start and end apart: 6 -> 6, of which waited for: 6 -> 4; matrix products, arithmetic and copies ran while one was open for 0% -> 3% of each run, Pallas kernels for 0% -> 0%
where the time goes in v1:
time: 247 us
  waiting for transfers between devices  88.8 us (36%)
  Pallas kernels  84.9 us (34%)
  other arithmetic  23.3 us (9%)
  blocking collectives  18.4 us (7%)
  between operations  13.4 us (5%)
  local copies, waits for them, and re-layouts  7.46 us (3%)
  starting transfers between devices  6.23 us (3%)
  matrix products  4.22 us (2%)
    pallas_call x1, Pallas kernels, mixer(): pl.pallas_call(functools.partial(mixer_kernel, sp_size, tp_size), out_sha...  84.9 us
    all_gather x1, waiting for transfers between devices, regroup_weights(): lax.all_gather(stacked, 'sp', axis=0, tiled=False, axis_index_groups=inne...  31.8 us
    all_gather x1, waiting for transfers between devices, regroup_weights(): lax.all_gather(down, 'sp', axis=0, tiled=True, axis_index_groups=inner_gr...  30.8 us
    ppermute x3, waiting for transfers between devices, regroup_weights(): piece = lax.ppermute(piece, 'sp', perm)  25.5 us
    all_gather x1, blocking collectives, carried_in(): gathered = jax.tree.map(lambda a: lax.all_gather(a, axis), part)  18.4 us
    dot_general x4, other arithmetic, block_update(): jnp.einsum('htk,hsk,htsk->hts', query_rows_block, gate_rows_block, decay_...  14.2 us
    ppermute x3, starting transfers between devices, regroup_weights(): piece = lax.ppermute(piece, 'sp', perm)  6.14 us
  transfers between devices with their start and end apart: 6, of which 4 were waited for; matrix products, arithmetic and copies ran while one was open for 3% of the time, Pallas kernels for 0%

profile of v1, /device:TPU:0, one launch (start us, length us, event | category | flops | bytes accessed | tf_op | source)
XLA Modules:
  0.0 247.1 jit_solution(466943781068980468)
XLA Ops:
  6.5 1.2 fusion.25
  7.7 0.1 reshape.119
  7.9 0.1 reshape.120
  8.0 1.0 reshape.130
  9.1 0.2 fusion.20
  9.4 1.0 bitcast_multiply_fusion.5
  10.4 0.1 reshape.122
  10.5 22.4 %while.26 = (s32[]{:T(128)}, f32[2,128,128]{2,1,0:T(8,128)S(1)}, f32[4,2,64,128]{3,2,0,1:T(8,128)S(1)}, f32[4,2,64,128]{3,1,2,0:T(2,128)S(1)}, f32[4,2,64,128]{3...) while((s32[]{:T(128)}, f32[2,128,128]{2,1,0:T(8,128)S(1)}, ...), condition=%wide.region_2.3_spmd.clone, body=%wide.region_0.2_spmd.clone.sunk | while | flops 69382144 | bytes 10729608 | solution.py:361
  10.6 0.1 reduce_window_sum.28
  10.7 0.2 fusion.36
  11.0 0.4 convolution_add_fusion.3
  11.4 0.8 select_exponential_fusion.2
  12.3 3.5 %fusion.37 = f32[2,64,64]{1,2,0:T(8,128)S(1)} fusion(f32[2,64,64,128]{3,2,1,0:T(8,128)S(1)} %select_exponential_fusion.2, f32[2,128,64]{1,2,0:T(8,128)S(1)} %bitcast.113, f32[2,128,64]{1,2,0:T(8,128)S(1)} %bitcast.114), kind=kLoop, calls=%fused_computation.4.clone.1 | loop fusion | flops 3137536 | bytes 4358144 | tf_op jit(solution)/shard_map/while/body/eval_jaxpr/htk,hsk,htsk->hts/dot_general | solution.py:45
  15.8 0.3 fusion.38
  16.3 0.2 fusion.36
  16.6 0.4 convolution_add_fusion.3
  17.0 0.8 select_exponential_fusion.2
  17.9 3.5 %fusion.37 = f32[2,64,64]{1,2,0:T(8,128)S(1)} fusion(f32[2,64,64,128]{3,2,1,0:T(8,128)S(1)} %select_exponential_fusion.2, f32[2,128,64]{1,2,0:T(8,128)S(1)} %bitcast.113, f32[2,128,64]{1,2,0:T(8,128)S(1)} %bitcast.114), kind=kLoop, calls=%fused_computation.4.clone.1 | loop fusion | flops 3137536 | bytes 4358144 | tf_op jit(solution)/shard_map/while/body/eval_jaxpr/htk,hsk,htsk->hts/dot_general | solution.py:45
  21.5 0.3 fusion.38
  21.9 0.2 fusion.36
  22.2 0.4 convolution_add_fusion.3
  22.6 0.8 select_exponential_fusion.2
  23.5 3.5 %fusion.37 = f32[2,64,64]{1,2,0:T(8,128)S(1)} fusion(f32[2,64,64,128]{3,2,1,0:T(8,128)S(1)} %select_exponential_fusion.2, f32[2,128,64]{1,2,0:T(8,128)S(1)} %bitcast.113, f32[2,128,64]{1,2,0:T(8,128)S(1)} %bitcast.114), kind=kLoop, calls=%fused_computation.4.clone.1 | loop fusion | flops 3137536 | bytes 4358144 | tf_op jit(solution)/shard_map/while/body/eval_jaxpr/htk,hsk,htsk->hts/dot_general | solution.py:45
  27.1 0.3 fusion.38
  27.5 0.2 fusion.36
  27.8 0.4 convolution_add_fusion.3
  28.2 0.8 select_exponential_fusion.2
  29.1 3.5 %fusion.37 = f32[2,64,64]{1,2,0:T(8,128)S(1)} fusion(f32[2,64,64,128]{3,2,1,0:T(8,128)S(1)} %select_exponential_fusion.2, f32[2,128,64]{1,2,0:T(8,128)S(1)} %bitcast.113, f32[2,128,64]{1,2,0:T(8,128)S(1)} %bitcast.114), kind=kLoop, calls=%fused_computation.4.clone.1 | loop fusion | flops 3137536 | bytes 4358144 | tf_op jit(solution)/shard_map/while/body/eval_jaxpr/htk,hsk,htsk->hts/dot_general | solution.py:45
  32.7 0.3 fusion.38
  33.0 0.6 copy-done
  33.8 0.1 dynamic-slice_bitcast_fusion
  33.9 5.1 %collective-permute-start.2 = (bf16[256,512]{1,0:T(8,128)(2,1)S(1)}, bf16[256,512]{1,0:T(8,128)(2,1)S(1)}, u32[]{:S(2)}, u32[]{:S(2)}) collective-permute-start(bf16[256,512]{1,0:T(8,128)(2,1)S(1)} %get-tuple-element.167), channel_id=1, source_target_pairs={{0,24},{4,28},{8,0},{12,4},{16,8},{20,12},{24,16},{28,20},{1,25},{... | collective-permute-start | bytes 786440 | tf_op jit(solution)/shard_map/ppermute | solution.py:329
  39.0 1.0 collective-permute-start
  40.0 6.4 %collective-permute-done.2 = bf16[256,512]{1,0:T(8,128)(2,1)S(1)} collective-permute-done((bf16[256,512]{1,0:T(8,128)(2,1)S(1)}, bf16[256,512]{1,0:T(8,128)(2,1)S(1)}, u32[]{:S(2)}, u32[]{:S(2)}) %collective-permute-start.2) | collective-permute-done | bytes 262176 | tf_op jit(solution)/shard_map/ppermute | solution.py:329
  46.5 19.1 %collective-permute-done.1 = bf16[256,512]{1,0:T(8,128)(2,1)S(1)} collective-permute-done((bf16[256,512]{1,0:T(8,128)(2,1)S(1)}, bf16[256,512]{1,0:T(8,128)(2,1)S(1)}, u32[]{:S(2)}, u32[]{:S(2)}) %collective-permute-start.1) | collective-permute-done | bytes 262176 | tf_op jit(solution)/shard_map/ppermute | solution.py:329
  65.6 1.1 pad_maximum_fusion
  66.7 0.7 all-gather.6.cloned.1.call-update
  67.6 0.1 copy.59
  67.7 0.1 copy.58
  67.8 18.4 %all_gather.18 = f32[8,2,128]{2,1,0:T(2,128)S(1)} all-gather(f32[1,2,128]{2,1,0:T(2,128)S(1)} %bitcast.135), channel_id=1, replica_groups=mesh['sp'=8,'tp'=4] {'sp'}, dimensions={0}, use_global_device_ids=true | all-gather | bytes 9216 | tf_op jit(solution)/shard_map/all_gather | solution.py:21
  86.2 0.4 multiply_reduce_fusion
  86.8 0.8 copy.69.mixed_ref
  87.6 31.8 %all-gather.10.cloned.1.call-done = bf16[8,256,512]{2,1,0:T(8,128)(2,1)} async-done(((bf16[4,256,512]{2,1,0:T(8,128)(2,1)}), bf16[8,256,512]{2,1,0:T(8,128)(2,1)}) %all-gather.10.cloned.1.call-update) | async-done | bytes 2097168 | tf_op jit(solution)/shard_map/all_gather | solution.py:332
  119.4 2.3 gather_fusion
  121.6 1.6 broadcast_select_fusion
  123.2 30.8 %all-gather.6.cloned.1.call-done.down_ref = bf16[512,2048]{1,0:T(8,128)(2,1)} async-done(((bf16[256,2048]{1,0:T(8,128)(2,1)}), bf16[512,2048]{1,0:T(8,128)(2,1)}) %all-gather.6.cloned.1.call-update) | async-done | bytes 2097168 | tf_op jit(solution)/shard_map/all_gather | solution.py:319
  154.0 84.9 %shard_map.118 = bf16[64,2048]{1,0:T(8,128)(2,1)} custom-call(bf16[256,256]{1,0:T(8,128)(2,1)} %copy.69.mixed_ref, bf16[256,2048]{1,0:T(8,128)(2,1)} %wo_ref.1, bf16[64,2048]{1,0:T(8,128)(2,1)} %res_ref.1, f32[1,2048]{1,0:T(1,128)} %bitcast.134, bf16[2048,512]{1,0:T(8,128)(2,1)} %bitcast.112, bf16[512,2048]{1,0:T(8,128)(2,1)} %all-gather.6.cloned.1.call-done.down_ref), custom_call_target="tpu_custom_call" | custom-call | tf_op jit(solution)/shard_map/pallas_call | solution.py:288
  238.9 1.7 copy.140
  (66 shorter events, 1.1 us)
Async XLA Ops:
  6.5 79.7 %all-gather.8.cloned.1.call-start = ((), (), s32[]{:S(2)}) async-start(), calls=%async_computation.1 | async-start | bytes 1179648 | tf_op jit(solution)/shard_map/all_gather | solution.py:21
  10.5 23.2 %copy-start.1 = (bf16[256,2048]{1,0:T(8,128)(2,1)S(1)}, bf16[256,2048]{1,0:T(8,128)(2,1)}, u32[]{:S(2)}) copy-start(bf16[256,2048]{1,0:T(8,128)(2,1)} %param.26) | copy-start | bytes 3145732
  33.0 0.7 copy-start
  33.0 34.5 %copy-start.2 = (bf16[256,256]{1,0:T(8,128)(2,1)S(1)}, bf16[256,256]{1,0:T(8,128)(2,1)}, u32[]{:S(2)}) copy-start(bf16[256,256]{1,0:T(8,128)(2,1)} %param.19) | copy-start | bytes 393220
  33.7 85.7 %all-gather.10.cloned.1.call-start = ((), (), s32[]{:S(2)}) async-start(), calls=%async_computation.2 | async-start | bytes 3145728 | tf_op jit(solution)/shard_map/all_gather | solution.py:332
  33.9 12.6 %collective-permute-start.2 = (bf16[256,512]{1,0:T(8,128)(2,1)S(1)}, bf16[256,512]{1,0:T(8,128)(2,1)S(1)}, u32[]{:S(2)}, u32[]{:S(2)}) collective-permute-start(bf16[256,512]{1,0:T(8,128)(2,1)S(1)} %get-tuple-element.167), channel_id=1, source_target_pairs={{0,24},{4,28},{8,0},{12,4},{16,8},{20,12},{24,16},{28,20},{1,25},{... | collective-permute-start | bytes 786440 | tf_op jit(solution)/shard_map/ppermute | solution.py:329
  39.0 26.5 %collective-permute-start.1 = (bf16[256,512]{1,0:T(8,128)(2,1)S(1)}, bf16[256,512]{1,0:T(8,128)(2,1)S(1)}, u32[]{:S(2)}, u32[]{:S(2)}) collective-permute-start(bf16[256,512]{1,0:T(8,128)(2,1)S(1)} %get-tuple-element.168), channel_id=1, source_target_pairs={{0,16},{4,20},{8,24},{12,28},{16,0},{20,4},{24,8},{28,12},{1,17},{... | collective-permute-start | bytes 786440 | tf_op jit(solution)/shard_map/ppermute | solution.py:329
  39.0 26.5 %collective-permute-start = (bf16[256,512]{1,0:T(8,128)(2,1)S(1)}, bf16[256,512]{1,0:T(8,128)(2,1)S(1)}, u32[]{:S(2)}, u32[]{:S(2)}) collective-permute-start(bf16[256,512]{1,0:T(8,128)(2,1)S(1)} %get-tuple-element.166), channel_id=1, source_target_pairs={{0,8},{4,12},{8,16},{12,20},{16,24},{20,28},{24,0},{28,4},{1,9},{5... | collective-permute-start | bytes 786440 | tf_op jit(solution)/shard_map/ppermute | solution.py:329
  65.6 21.1 %copy-start.3 = (f32[128]{0:T(128)S(1)}, f32[128]{0:T(128)}, u32[]{:S(2)}) copy-start(f32[128]{0:T(128)} %param.22) | copy-start | bytes 1540
  66.7 87.3 %all-gather.6.cloned.1.call-start = ((), (), s32[]{:S(2)}) async-start(), calls=%async_computation | async-start | bytes 3145728 | tf_op jit(solution)/shard_map/all_gather | solution.py:319
Sparse Core Ops, SparseCore 0:
  33.8 52.3 all-gather.7
  87.7 31.6 all-gather.9
  120.9 33.0 all-gather.5

commit v2 on v1

v2 whole, which is shorter than its diff:
```python
import functools

import jax
import jax.numpy as jnp
from jax import lax
from jax.experimental import pallas as pl
from jax.experimental.pallas import tpu as pltpu
from jax.sharding import PartitionSpec as P

HEAD_K = 128
HEAD_V = 128
BLOCK = 64


norm_eps = 1e-06
highest_precision = lax.Precision.HIGHEST


OUTER = 4
LO = 2
MESH = pl.DeviceIdType.MESH


def layer_kernel(
    sp_size, tp_size,
    q_ref, f_ref, v_ref, g_ref, gap_ref, ex_ref, hg_ref,
    wo_ref, res_ref, gain_ref, upsh_ref, downsh_ref, out_ref,
    upbuf, downbuf, rec, qrun, mixed_ref, ins, int_, outs, outt,
    pbuf, stream, s5, r5, s6, r6, nb, acc, s1, r1, s2, r2, acc2, s3, r3,
    sem5s, sem5r, sem6s, sem6r, zs, zr, hs, hr, ls, lr, ls2, lr2,
    q1s, q1r, q2s, q2r, q3s, q3r,
    wl, wzs, wzr, wxs, wxr, wds, wdr, iss, isr, its, itr, oss, osr, ots, otr,
):
    outer, inner, hi = OUTER, sp_size // OUTER, tp_size // LO
    sp, tp = lax.axis_index("sp"), lax.axis_index("tp")
    o, i = lax.div(sp, inner), lax.rem(sp, inner)
    h, l = lax.div(tp, LO), lax.rem(tp, LO)
    other = 1 - l
    rows, depth = res_ref.shape

    def dev(oo, hh, ll):
        return (oo * inner + i, hh * LO + ll)

    def at_i(j):
        return (o * inner + lax.rem(i + j, inner), tp)

    def at_o(k):
        return lax.rem(o + k, outer)

    def from_o(k):
        return lax.rem(o - k + outer, outer)

    def at_h(m):
        return lax.rem(h + m, hi)

    def from_h(m):
        return lax.rem(h - m + hi, hi)

    def rcopy(src, dst, ssem, rsem, device):
        return pltpu.make_async_remote_copy(
            src_ref=src, dst_ref=dst, send_sem=ssem, recv_sem=rsem,
            device_id=device, device_id_type=MESH,
        )

    barrier = pltpu.get_barrier_semaphore()
    peers = [dev(at_o(k), h, l) for k in range(1, outer)]
    peers += [dev(o, at_h(m), l) for m in range(1, hi)] + [dev(o, h, other)]
    peers += [at_i(j) for j in range(1, inner)]
    for peer in peers:
        pl.semaphore_signal(barrier, inc=1, device_id=peer, device_id_type=MESH)
    pl.semaphore_wait(barrier, len(peers))

    width = upbuf.shape[2]

    def up_piece(to):
        return upsh_ref.at[:, pl.ds(pl.multiple_of(to * width, width), width)]

    def wz_copy(k):
        return rcopy(up_piece(at_o(k)), upbuf.at[sp], wzs.at[k], wzr.at[k], dev(at_o(k), h, l))

    def wx_copy(k, j):
        ref = upbuf.at[from_o(k) * inner + i]
        return rcopy(ref, ref, wxs.at[k, j], wxr.at[k, j], at_i(j))

    def wd_copy(j):
        return rcopy(downsh_ref, downbuf.at[i], wds.at[j], wdr.at[j], at_i(j))

    own_up = pltpu.make_async_copy(up_piece(o), upbuf.at[sp], wl.at[0])
    own_down = pltpu.make_async_copy(downsh_ref, downbuf.at[i], wl.at[1])
    for k in range(1, outer):
        wz_copy(k).start()
    for j in range(1, inner):
        wd_copy(j).start()
    own_up.start()
    own_down.start()

    length = q_ref.shape[0]
    heads = q_ref.shape[1] // HEAD_K
    row_at = lax.broadcasted_iota(jnp.int32, (BLOCK, BLOCK), 0)
    col_at = lax.broadcasted_iota(jnp.int32, (BLOCK, BLOCK), 1)
    causal = row_at >= col_at
    lower = causal.astype(jnp.float32)

    def dot(a, b, dims):
        return lax.dot_general(
            a, b, (dims, ((), ())), precision=highest_precision,
            preferred_element_type=jnp.float32,
        )

    states = [jnp.zeros((HEAD_V, HEAD_K), jnp.float32) for _ in range(heads)]
    before = jnp.zeros((1, q_ref.shape[1]), jnp.float32)
    for b in range(length // BLOCK):
        at = pl.ds(b * BLOCK, BLOCK)
        gate = gap_ref[...] * (1.0 / (1.0 + jnp.exp(f_ref[at, :].astype(jnp.float32))))
        rate = jnp.log1p(-gate) + ex_ref[at, :]
        cum = dot(lower, rate, ((1,), (0,)))
        last = cum[BLOCK - 1 : BLOCK, :]
        qe = q_ref[at, :].astype(jnp.float32) * HEAD_K ** (-0.5) * jnp.exp(cum)
        ke = gate * jnp.exp(-cum)
        kd = gate * jnp.exp(last - cum)
        keep = jnp.exp(last)
        qrun[at, :] = qe * jnp.exp(before)
        before = before + last
        for n in range(heads):
            lane = slice(n * HEAD_K, (n + 1) * HEAD_K)
            val = v_ref[at, lane].astype(jnp.float32)
            scores = dot(qe[:, lane], ke[:, lane], ((1,), (1,)))
            scores = jnp.where(causal, scores, 0.0)
            got = dot(scores, val, ((1,), (0,)))
            if b:
                got = got + dot(qe[:, lane], states[n], ((1,), (1,)))
            rec[at, lane] = got
            fresh = dot(val, kd[:, lane], ((0,), (0,)))
            states[n] = states[n] * keep[:, lane] + fresh

    def is_copy(j):
        return rcopy(ins.at[i], ins.at[i], iss.at[j], isr.at[j], at_i(j))

    def it_copy(j):
        return rcopy(int_.at[i], int_.at[i], its.at[j], itr.at[j], at_i(j))

    def os_copy(k):
        return rcopy(outs.at[o], outs.at[o], oss.at[k], osr.at[k], dev(at_o(k), h, l))

    def ot_copy(k):
        return rcopy(outt.at[o], outt.at[o], ots.at[k], otr.at[k], dev(at_o(k), h, l))

    for n in range(heads):
        ins[i, n] = states[n].astype(jnp.bfloat16)
    int_[i] = jnp.broadcast_to(before, int_.shape[1:])
    for j in range(1, inner):
        is_copy(j).start()
        it_copy(j).start()
    for j in range(1, inner):
        is_copy(j).wait_recv()
        it_copy(j).wait_recv()

    def fold(carry, state_ref, log_ref, at, use):
        logs, parts = carry
        log = log_ref[at][0:1, :]
        keep = jnp.exp(log)
        new = []
        for n in range(heads):
            lane = slice(n * HEAD_K, (n + 1) * HEAD_K)
            step = parts[n] * keep[:, lane] + state_ref[at, n].astype(jnp.float32)
            new.append(step if use is None else jnp.where(use, step, parts[n]))
        both = logs + log
        return (both if use is None else jnp.where(use, both, logs), new)

    nothing = (
        jnp.zeros((1, q_ref.shape[1]), jnp.float32),
        [jnp.zeros((HEAD_V, HEAD_K), jnp.float32) for _ in range(heads)],
    )
    group, inner_part = nothing, nothing
    for j in range(inner):
        group = fold(group, ins, int_, j, None)
        inner_part = fold(inner_part, ins, int_, j, j < i)
    for n in range(heads):
        outs[o, n] = group[1][n].astype(jnp.bfloat16)
    outt[o] = jnp.broadcast_to(group[0], outt.shape[1:])
    for k in range(1, outer):
        os_copy(k).start()
        ot_copy(k).start()
    own_up.wait()
    for k in range(outer):
        if k:
            wz_copy(k).wait_recv()
        for j in range(1, inner):
            wx_copy(k, j).start()
    for k in range(1, outer):
        os_copy(k).wait_recv()
        ot_copy(k).wait_recv()
    arrived = nothing
    for k in range(outer):
        arrived = fold(arrived, outs, outt, k, k < o)
    inner_keep = jnp.exp(inner_part[0])
    for n in range(heads):
        lane = slice(n * HEAD_K, (n + 1) * HEAD_K)
        came = arrived[1][n] * inner_keep[:, lane] + inner_part[1][n]
        out = rec[:, lane] + dot(qrun[:, lane], came, ((1,), (1,)))
        out = out * lax.rsqrt(jnp.mean(out * out, axis=-1, keepdims=True) + norm_eps)
        logit = g_ref[:, lane].astype(jnp.float32)
        gating = logit / (1.0 + jnp.exp(-logit))
        mixed_ref[:, lane] = (out * hg_ref[...] * gating).astype(jnp.bfloat16)

    branch = jnp.dot(mixed_ref[...], wo_ref[...], preferred_element_type=jnp.float32)
    pbuf[...] = branch.reshape(tp_size, rows, depth)
    for hh in range(hi):
        s5[hh] = pbuf[hh * LO + other].astype(jnp.bfloat16)
    c5 = rcopy(s5, r5, sem5s, sem5r, dev(o, h, other))
    c5.start()
    c5.wait_recv()
    c6 = []
    for m in range(1, hi):
        to = at_h(m)
        s6[m] = (pbuf[to * LO + l] + r5[to].astype(jnp.float32)).astype(jnp.bfloat16)
        c = rcopy(s6.at[m], r6.at[m], sem6s.at[m], sem6r.at[m], dev(o, to, l))
        c.start()
        c6.append(c)
    total = pbuf[tp] + r5[h].astype(jnp.float32) + res_ref[...].astype(jnp.float32)
    for m in range(1, hi):
        c6[m - 1].wait_recv()
        total = total + r6[m].astype(jnp.float32)
    stream[...] = total
    scale = lax.rsqrt(jnp.mean(total * total, axis=-1, keepdims=True) + norm_eps)
    nb[o, tp] = (total * scale * gain_ref[...]).astype(jnp.bfloat16)

    def z_copy(k):
        return rcopy(nb.at[o, tp], nb.at[o, tp], zs.at[k], zr.at[k], dev(at_o(k), h, l))

    def h_copy(k, m):
        ref = nb.at[from_o(k), tp]
        return rcopy(ref, ref, hs.at[k, m], hr.at[k, m], dev(o, at_h(m), l))

    def l_copy(k):
        ref = nb.at[from_o(k), tp]
        return rcopy(ref, ref, ls.at[k], lr.at[k], dev(o, h, other))

    def l2_copy(k, m):
        ref = nb.at[from_o(k), from_h(m) * LO + l]
        return rcopy(ref, ref, ls2.at[k, m], lr2.at[k, m], dev(o, h, other))

    def s1_copy(k):
        return rcopy(s1.at[k], r1.at[k], q1s.at[k], q1r.at[k], dev(o, h, other))

    def s2_copy(k, m):
        return rcopy(s2.at[k, m], r2.at[k, m], q2s.at[k, m], q2r.at[k, m], dev(o, at_h(m), l))

    def s3_copy(k):
        return rcopy(s3.at[k], r3.at[k], q3s.at[k], q3r.at[k], dev(from_o(k), h, l))

    for k in range(1, outer):
        z_copy(k).start()

    def forward(k):
        for m in range(1, hi):
            h_copy(k, m).start()
        l_copy(k).start()

    forward(0)
    own_down.wait()
    for j in range(1, inner):
        wd_copy(j).wait_recv()
        for k in range(outer):
            wx_copy(k, j).wait_recv()

    def body(j, carry):
        @pl.when(j + 1 < outer)
        def _():
            z_copy(j + 1).wait_recv()
            forward(j + 1)

        @pl.when(j < outer)
        def _():
            for m in range(1, hi):
                h_copy(j, m).wait_recv()
                l2_copy(j, m).start()
            l_copy(j).wait_recv()
            for m in range(1, hi):
                l2_copy(j, m).wait_recv()
            x = nb[from_o(j)].reshape(tp_size * rows, depth)
            lifted = jnp.dot(x, upbuf[...].reshape(depth, width), preferred_element_type=jnp.float32)
            hidden = jnp.square(jnp.maximum(lifted, 0.0)).astype(jnp.bfloat16)
            part = jnp.dot(hidden, downbuf[...].reshape(width, depth), preferred_element_type=jnp.float32)
            pbuf[...] = part.reshape(tp_size, rows, depth)
            for hh in range(hi):
                s1[j, hh] = pbuf[hh * LO + other].astype(jnp.bfloat16)
            s1_copy(j).start()
            for hh in range(hi):
                acc[j, hh] = pbuf[hh * LO + l]

        @pl.when((j >= 1) & (j < outer + 1))
        def _():
            k = j - 1
            s1_copy(k).wait_recv()
            for m in range(1, hi):
                to = at_h(m)
                s2[k, m] = (acc[k, to] + r1[k, to].astype(jnp.float32)).astype(jnp.bfloat16)
                s2_copy(k, m).start()
            acc2[k] = acc[k, h] + r1[k, h].astype(jnp.float32)

        @pl.when(j >= 2)
        def _():
            k = j - 2
            v = acc2[k]
            for m in range(1, hi):
                s2_copy(k, m).wait_recv()
                v = v + r2[k, m].astype(jnp.float32)
            @pl.when(k == 0)
            def _():
                acc2[0] = v

            @pl.when(k > 0)
            def _():
                s3[k] = v.astype(jnp.bfloat16)
                s3_copy(k).start()

        return carry

    lax.fori_loop(0, outer + 2, body, 0)
    final = stream[...] + acc2[0]
    for k in range(1, outer):
        s3_copy(k).wait_recv()
        final = final + r3[k].astype(jnp.float32)
    out_ref[...] = final.astype(jnp.bfloat16)

    for k in range(1, outer):
        wz_copy(k).wait_send()
        os_copy(k).wait_send()
        ot_copy(k).wait_send()
    for j in range(1, inner):
        wd_copy(j).wait_send()
        is_copy(j).wait_send()
        it_copy(j).wait_send()
        for k in range(outer):
            wx_copy(k, j).wait_send()
    c5.wait_send()
    for c in c6:
        c.wait_send()
    for k in range(outer):
        if k > 0:
            z_copy(k).wait_send()
            s3_copy(k).wait_send()
        l_copy(k).wait_send()
        s1_copy(k).wait_send()
        for m in range(1, hi):
            h_copy(k, m).wait_send()
            l2_copy(k, m).wait_send()
            s2_copy(k, m).wait_send()


def on_device(
    sp_size, tp_size,
    query, forget_logits, written_values, output_gate_logits, forget_floor_gap,
    extra_log_decay, head_norm_gain, output_weight, residual, mixer_norm_gain,
    mixer_up_weight, mixer_down_weight,
):
    rows, depth = residual.shape
    length, wide = query.shape
    heads = wide // HEAD_K
    hi = tp_size // LO
    f32, b16 = jnp.float32, jnp.bfloat16
    dma = pltpu.SemaphoreType.DMA
    vm = pltpu.VMEM
    O = OUTER
    inner = sp_size // O
    part, cols = mixer_up_weight.shape
    width = cols // O
    return pl.pallas_call(
        functools.partial(layer_kernel, sp_size, tp_size),
        out_shape=jax.ShapeDtypeStruct((rows, depth), b16),
        in_specs=[pl.BlockSpec(memory_space=pltpu.VMEM)] * 12,
        out_specs=pl.BlockSpec(memory_space=pltpu.VMEM),
        scratch_shapes=[
            vm((sp_size, part, width), b16), vm((inner,) + mixer_down_weight.shape, b16),
            vm((length, wide), f32), vm((length, wide), f32), vm((length, wide), b16),
            vm((inner, heads, HEAD_V, HEAD_K), b16), vm((inner, 8, wide), f32),
            vm((O, heads, HEAD_V, HEAD_K), b16), vm((O, 8, wide), f32),
            vm((tp_size, rows, depth), f32),
            vm((rows, depth), f32),
            vm((hi, rows, depth), b16), vm((hi, rows, depth), b16),
            vm((hi, rows, depth), b16), vm((hi, rows, depth), b16),
            vm((O, tp_size, rows, depth), b16),
            vm((O, hi, rows, depth), f32),
            vm((O, hi, rows, depth), b16), vm((O, hi, rows, depth), b16),
            vm((O, hi, rows, depth), b16), vm((O, hi, rows, depth), b16),
            vm((O, rows, depth), f32),
            vm((O, rows, depth), b16), vm((O, rows, depth), b16),
            dma, dma, dma((hi,)), dma((hi,)),
            dma((O,)), dma((O,)), dma((O, hi)), dma((O, hi)),
            dma((O,)), dma((O,)), dma((O, hi)), dma((O, hi)),
            dma((O,)), dma((O,)), dma((O, hi)), dma((O, hi)),
            dma((O,)), dma((O,)),
            dma((2,)), dma((O,)), dma((O,)), dma((O, inner)), dma((O, inner)),
            dma((inner,)), dma((inner,)),
            dma((inner,)), dma((inner,)), dma((inner,)), dma((inner,)),
            dma((O,)), dma((O,)), dma((O,)), dma((O,)),
        ],
        compiler_params=pltpu.CompilerParams(
            collective_id=0, has_side_effects=True, vmem_limit_bytes=60 * 1024 * 1024
        ),
    )(
        query, forget_logits, written_values, output_gate_logits,
        forget_floor_gap.reshape(1, wide), extra_log_decay, head_norm_gain.reshape(1, HEAD_V),
        output_weight, residual, mixer_norm_gain.reshape(1, depth),
        mixer_up_weight, mixer_down_weight,
    )


def solution(mesh):
    return jax.shard_map(
        functools.partial(on_device, mesh.shape["sp"], mesh.shape["tp"]),
        mesh=mesh,
        in_specs=(
            P("sp", "tp"),
            P("sp", "tp"),
            P("sp", "tp"),
            P("sp", "tp"),
            P("tp"),
            P("sp", "tp"),
            P(),
            P("tp", None),
            P(("sp", "tp"), None),
            P(),
            P("sp", "tp"),
            P(("tp", "sp"), None),
        ),
        out_specs=P(("sp", "tp"), None),
        check_vma=False,
    )
```

time: 247 us -> 127 us (0.51)
  waiting for transfers between devices: 88.8 us -> 0 us
  Pallas kernels: 84.9 us -> 125 us
  other arithmetic: 23.3 us -> 0 us
  blocking collectives: 18.4 us -> 0 us
  between operations: 13.4 us -> 0.01 us
  starting transfers between devices: 6.23 us -> 0 us
  local copies, waits for them, and re-layouts: 7.46 us -> 1.67 us
  matrix products: 4.22 us -> 0 us
    all_gather x3 -> x0, waiting for transfers between devices: 62.6 us -> none  [the longest x1 31.8 us: regroup_weights(): lax.all_gather(stacked, 'sp', axis=0, tiled=False, axis_index_groups=inne...]
    pallas_call x1, Pallas kernels: 84.9 us -> 125 us  [on_device(): pl.pallas_call(functools.partial(layer_kernel, sp_size, tp_size), out_sha...]
    ppermute x3 -> x0, waiting for transfers between devices: 25.5 us -> none  [regroup_weights(): piece = lax.ppermute(piece, 'sp', perm)]
    all_gather x1 -> x0, blocking collectives: 18.4 us -> none  [carried_in(): gathered = jax.tree.map(lambda a: lax.all_gather(a, axis), part)]
    dot_general x4 -> x0, other arithmetic: 14.2 us -> none  [block_update(): jnp.einsum('htk,hsk,htsk->hts', query_rows_block, gate_rows_block, decay_...]
    ppermute x3 -> x0, starting transfers between devices: 6.14 us -> none  [regroup_weights(): piece = lax.ppermute(piece, 'sp', perm)]
    dot_general x13 -> x0, matrix products: 4.22 us -> none  [the longest x4 1.62 us: block_update(): jnp.einsum('tri,trw->tiw', gate_rows_block * jnp.exp(final_log_total - cu...]
    exp x5 -> x0, other arithmetic: 3.41 us -> none  [the longest x4 3.36 us: block_update(): decay_table = jnp.exp(jnp.where(causal[None, :, :, None], spread, -jnp.inf))]
  transfers between devices with their start and end apart: 6 -> 0, of which waited for: 4 -> 0; matrix products, arithmetic and copies ran while one was open for 3% -> 0% of each run, Pallas kernels for 0% -> 0%
where the time goes in v2:
time: 127 us; the launch traced here: 126 us
  Pallas kernels  125 us (98%)
  local copies, waits for them, and re-layouts  1.67 us (1%)
    pallas_call x1, Pallas kernels, on_device(): pl.pallas_call(functools.partial(layer_kernel, sp_size, tp_size), out_sha...  125 us

profile of v2, /device:TPU:0, one launch (start us, length us, event | category | flops | bytes accessed | tf_op | source)
XLA Modules:
  0.0 126.3 jit_solution(16944107689485584431)
XLA Ops:
  0.0 124.6 %shard_map.118 = bf16[64,2048]{1,0:T(8,128)(2,1)} custom-call(bf16[256,256]{1,0:T(8,128)(2,1)} %q_ref.1, bf16[256,256]{1,0:T(8,128)(2,1)} %f_ref.1, bf16[256,256]{1,0:T(8,128)(2,1)} %v_ref.1, bf16[256,256]{1,0:T(8,128)(2,1)} %g_ref.1, f32[1,256]{1,0:T(1,128)} %bitcast.4, f32[256,256]{1,0:T(8,128)} %ex_ref.1, f32[1,128]{1,0:T(1,128)} %bitcast.5, ...), custom_call_target="tpu_custom_call" | custom-call | tf_op jit(solution)/shard_map/pallas_call | solution.py:369
  124.6 1.7 %copy.14 = bf16[64,2048]{1,0:T(8,128)(2,1)} copy(bf16[64,2048]{1,0:T(8,128)(2,1)} %shard_map.118) | data formatting | bytes 524288

commit v3 on v2

--- a/solution.py
+++ b/solution.py
@@ -82,15 +82,18 @@
         ref = upbuf.at[from_o(k) * inner + i]
         return rcopy(ref, ref, wxs.at[k, j], wxr.at[k, j], at_i(j))
 
-    def wd_copy(j):
-        return rcopy(downsh_ref, downbuf.at[i], wds.at[j], wdr.at[j], at_i(j))
+    half = downsh_ref.shape[0] // 2
+
+    def wd_copy(j, p):
+        some = pl.ds(p * half, half)
+        return rcopy(
+            downsh_ref.at[some], downbuf.at[i, some], wds.at[j, p], wdr.at[j, p], at_i(j)
+        )
 
     own_up = pltpu.make_async_copy(up_piece(o), upbuf.at[sp], wl.at[0])
     own_down = pltpu.make_async_copy(downsh_ref, downbuf.at[i], wl.at[1])
-    for k in range(1, outer):
-        wz_copy(k).start()
-    for j in range(1, inner):
-        wd_copy(j).start()
+    wz_copy(1).start()
+    wz_copy(2).start()
     own_up.start()
     own_down.start()
 
@@ -152,6 +155,10 @@
         is_copy(j).start()
         it_copy(j).start()
     for j in range(1, inner):
+        wd_copy(j, 1).start()
+    for j in range(1, inner):
+        wd_copy(j, 0).start()
+    for j in range(1, inner):
         is_copy(j).wait_recv()
         it_copy(j).wait_recv()
 
@@ -181,10 +188,11 @@
     for k in range(1, outer):
         os_copy(k).start()
         ot_copy(k).start()
+    for k in range(3, outer):
+        wz_copy(k).start()
     own_up.wait()
-    for k in range(outer):
-        if k:
-            wz_copy(k).wait_recv()
+    wz_copy(1).wait_recv()
+    for k in range(2):
         for j in range(1, inner):
             wx_copy(k, j).start()
     for k in range(1, outer):
@@ -258,9 +266,14 @@
         l_copy(k).start()
 
     forward(0)
+    for k in range(2, outer):
+        wz_copy(k).wait_recv()
+        for j in range(1, inner):
+            wx_copy(k, j).start()
     own_down.wait()
     for j in range(1, inner):
-        wd_copy(j).wait_recv()
+        for p in range(2):
+            wd_copy(j, p).wait_recv()
         for k in range(outer):
             wx_copy(k, j).wait_recv()
 
@@ -329,7 +342,8 @@
         os_copy(k).wait_send()
         ot_copy(k).wait_send()
     for j in range(1, inner):
-        wd_copy(j).wait_send()
+        for p in range(2):
+            wd_copy(j, p).wait_send()
         is_copy(j).wait_send()
         it_copy(j).wait_send()
         for k in range(outer):
@@ -392,7 +406,7 @@
             dma((O,)), dma((O,)), dma((O, hi)), dma((O, hi)),
             dma((O,)), dma((O,)),
             dma((2,)), dma((O,)), dma((O,)), dma((O, inner)), dma((O, inner)),
-            dma((inner,)), dma((inner,)),
+            dma((inner, 2)), dma((inner, 2)),
             dma((inner,)), dma((inner,)), dma((inner,)), dma((inner,)),
             dma((O,)), dma((O,)), dma((O,)), dma((O,)),
         ],

time: 127 us -> 118 us (0.929)
  Pallas kernels: 125 us -> 116 us
    pallas_call x1, Pallas kernels: 125 us -> 116 us  [on_device(): pl.pallas_call(functools.partial(layer_kernel, sp_size, tp_size), out_sha...]
where the time goes in v3:
time: 118 us; the launch traced here: 117 us
  Pallas kernels  116 us (98%)
  local copies, waits for them, and re-layouts  1.67 us (1%)
    pallas_call x1, Pallas kernels, on_device(): pl.pallas_call(functools.partial(layer_kernel, sp_size, tp_size), out_sha...  116 us

profile of v3, /device:TPU:0, one launch (start us, length us, event | category | flops | bytes accessed | tf_op | source)
XLA Modules:
  0.0 117.5 jit_solution(9314345800927893665)
XLA Ops:
  0.0 115.8 %shard_map.118 = bf16[64,2048]{1,0:T(8,128)(2,1)} custom-call(bf16[256,256]{1,0:T(8,128)(2,1)} %q_ref.1, bf16[256,256]{1,0:T(8,128)(2,1)} %f_ref.1, bf16[256,256]{1,0:T(8,128)(2,1)} %v_ref.1, bf16[256,256]{1,0:T(8,128)(2,1)} %g_ref.1, f32[1,256]{1,0:T(1,128)} %bitcast.4, f32[256,256]{1,0:T(8,128)} %ex_ref.1, f32[1,128]{1,0:T(1,128)} %bitcast.5, ...), custom_call_target="tpu_custom_call" | custom-call | tf_op jit(solution)/shard_map/pallas_call | solution.py:383
  115.8 1.7 %copy.14 = bf16[64,2048]{1,0:T(8,128)(2,1)} copy(bf16[64,2048]{1,0:T(8,128)(2,1)} %shard_map.118) | data formatting | bytes 524288
